TPU v7x, 32 devices: a whole 2x2x4 slice. The times are simulated.
32 devices in a mesh: dp: 4 (over y, x), kv: 4 (over z), tp: 2 (over core).
Axes of the slice: x: 2, y: 2, z: 4, core: 2. Of those that a mesh axis runs over, the one named last changes fastest.
Arguments:
- tokens: bfloat16 [4, 16, 2048], P('dp', None, 'kv'), may hold values from -18 to 18, as said below
- norm_gain: float32 [2048], P('kv'), may hold values from 0.1 to 1.9
- w_query: bfloat16 [2048, 3072], P('kv', 'tp'), may hold values from -0.125 to 0.125
- w_key: bfloat16 [2048, 3072], P('kv', 'tp'), may hold values from -0.125 to 0.125
- w_value: bfloat16 [2048, 3072], P('kv', 'tp'), may hold values from -0.125 to 0.125
- w_gate: bfloat16 [2048, 3072], P('kv', 'tp'), may hold values from -0.125 to 0.125
- w_out: bfloat16 [3072, 2048], P('tp', 'kv'), may hold values from -0.109375 to 0.109375
- head_bias: float32 [24], P('tp'), may hold values from -14 to -2
- cache_keys: bfloat16 [4, 2048, 24, 128], P('dp', 'kv', 'tp'), may hold values from -18 to 18, as said below
- cache_values: bfloat16 [4, 2048, 24, 128], P('dp', 'kv', 'tp'), may hold values from -6 to 6
- prefix_len: int32 [4], P('dp'), may hold values from 1536 to 2028
- accepted: int32 [4], P('dp'), may hold values from 1 to 4
- parent: int32 [4, 16], P('dp'), may hold values from -1 to 14, as said below
Outputs:
- mixed: bfloat16 [4, 16, 2048], P('dp', None, 'kv')
- keys_next: bfloat16 [4, 2048, 24, 128], P('dp', 'kv', 'tp')
- values_next: bfloat16 [4, 2048, 24, 128], P('dp', 'kv', 'tp')
Inputs may be any that keep to these rules, and one draw needn't show every extreme that they name: `tokens`: entries of order one. `cache_keys`: entries of order one. parent of proposal 0 is -1; for p of 1 or more, parent[p] lies in max(p - 3, 0) to p - 1.
All inputs are finite; a program needn't handle non-finite values.
Results may differ from a plain program's by a relative error of at most 0.012.
Values may be sent and summed in bfloat16 or wider, within the bound.
A program may use at most 64 MiB of HBM per device.

v0:
```python
import jax
import jax.numpy as jnp
from jax import lax
from jax.sharding import PartitionSpec as P

D = 2048
HEAD = 128
EPS = 1e-06


def ancestry(parent):
    count = parent.shape[-1]
    places = jnp.arange(count, dtype=jnp.int32)
    reach = (parent[:, :, None] == places[None, None, :]).astype(jnp.float32)
    for repeat in range(count.bit_length()):
        reach = jnp.minimum(
            reach + jnp.einsum("spj,sjk->spk", reach, reach, precision=lax.Precision.HIGHEST), 1.0
        )
    return reach > 0.5


def after_table(count):
    places = jnp.arange(count, dtype=jnp.int32)
    return (places[:, None] > places[None, :]).astype(jnp.float32)


def sum_after(values):
    table = after_table(values.shape[-1])
    return jnp.einsum("shpk,kc->shpc", values, table, precision=lax.Precision.HIGHEST)


def local(
    tokens,
    norm_gain,
    w_query,
    w_key,
    w_value,
    w_gate,
    w_out,
    head_bias,
    cache_keys,
    cache_values,
    prefix_len,
    accepted,
    parent,
):
    seqs, props, columns = tokens.shape
    width = w_query.shape[1]
    heads = width // HEAD
    flat = tokens.astype(jnp.float32).reshape(seqs * props, columns)
    square_part = jnp.sum(flat * flat, axis=1)
    scaled = (flat * norm_gain).astype(jnp.bfloat16)
    partial_value = jnp.concatenate(
        [
            jnp.dot(scaled, weight, preferred_element_type=jnp.float32)
            for weight in (w_query, w_key, w_value, w_gate)
        ],
        axis=1,
    )
    squares = lax.psum(square_part, "kv")
    share = lax.psum_scatter(partial_value, "kv", scatter_dimension=1, tiled=True)
    rscale = lax.rsqrt(squares / D + EPS)
    projected = lax.all_gather(
        (share * rscale[:, None]).astype(jnp.bfloat16), "kv", axis=1, tiled=True
    )
    shaped = projected.reshape(seqs, props, 4, heads, HEAD)
    query = shaped[:, :, 0]
    key_new = shaped[:, :, 1]
    value_new = shaped[:, :, 2]
    gate = projected[:, 3 * width :].astype(jnp.float32)
    factor = HEAD ** (-0.5)
    bias_col = head_bias[None, :, None, None]
    ctx_dev = cache_keys.shape[1]
    places = lax.axis_index("kv") * ctx_dev + jnp.arange(ctx_dev, dtype=jnp.int32)
    valid = prefix_len + accepted
    live = (places[None, :] < valid[:, None])[:, None, None, :]
    scores = (
        jnp.einsum("sphd,schd->shpc", query, cache_keys, preferred_element_type=jnp.float32)
        * factor
        + bias_col
    )
    keep_log = jnp.where(live, jax.nn.log_sigmoid(-scores), 0.0)
    shard_rest = jnp.sum(keep_log, axis=3)
    family = ancestry(parent)[:, None]
    tree_scores = (
        jnp.einsum("sphd,sjhd->shpj", query, key_new, preferred_element_type=jnp.float32) * factor
        + bias_col
    )
    tree_keep = jnp.where(family, jax.nn.log_sigmoid(-tree_scores), 0.0)
    tail = jnp.sum(tree_keep, axis=3)
    every = lax.all_gather(shard_rest[None], "kv", axis=0, tiled=True)
    after = jnp.arange(every.shape[0], dtype=jnp.int32) > lax.axis_index("kv")
    beyond = jnp.sum(jnp.where(after[:, None, None, None], every, 0.0), axis=0)
    later_cache = sum_after(keep_log) + (beyond + tail)[..., None]
    cache_weight = jnp.where(live, jnp.exp(jax.nn.log_sigmoid(scores) + later_cache), 0.0).astype(
        jnp.bfloat16
    )
    later_tree = sum_after(tree_keep)
    tree_weight = jnp.where(
        family, jnp.exp(jax.nn.log_sigmoid(tree_scores) + later_tree), 0.0
    ).astype(jnp.bfloat16)
    local_sum = jnp.einsum(
        "shpc,schd->sphd", cache_weight, cache_values, preferred_element_type=jnp.float32
    )
    attended = lax.psum(local_sum, "kv")
    attended = attended + jnp.einsum(
        "shpj,sjhd->sphd", tree_weight, value_new, preferred_element_type=jnp.float32
    )
    mixin = (attended.reshape(seqs * props, width) * jax.nn.silu(gate)).astype(jnp.bfloat16)
    part_out = jnp.dot(mixin, w_out, preferred_element_type=jnp.float32).astype(jnp.bfloat16)
    part_out = lax.optimization_barrier(part_out).astype(jnp.float32)
    mixed = lax.psum(part_out.astype(jnp.bfloat16), "tp").reshape(seqs, props, w_out.shape[1])
    relative = places[None, :] - valid[:, None]
    picker = (relative[:, :, None] == jnp.arange(props, dtype=jnp.int32)[None, None, :]).astype(
        jnp.bfloat16
    )
    inside = ((relative >= 0) & (relative < props))[:, :, None, None]
    placed_keys = jnp.einsum(
        "scp,sphd->schd", picker, key_new, preferred_element_type=jnp.float32
    ).astype(jnp.bfloat16)
    placed_values = jnp.einsum(
        "scp,sphd->schd", picker, value_new, preferred_element_type=jnp.float32
    ).astype(jnp.bfloat16)
    keys_next = jnp.where(inside, placed_keys, cache_keys)
    values_next = jnp.where(inside, placed_values, cache_values)
    return (mixed, keys_next, values_next)


def solution(mesh):
    return jax.shard_map(
        local,
        mesh=mesh,
        in_specs=(
            P("dp", None, "kv"),
            P("kv"),
            P("kv", "tp"),
            P("kv", "tp"),
            P("kv", "tp"),
            P("kv", "tp"),
            P("tp", "kv"),
            P("tp"),
            P("dp", "kv", "tp", None),
            P("dp", "kv", "tp", None),
            P("dp"),
            P("dp"),
            P("dp", None),
        ),
        out_specs=(P("dp", None, "kv"), P("dp", "kv", "tp", None), P("dp", "kv", "tp", None)),
        check_vma=False,
    )
```

profile of v0, /device:TPU:0, one launch (start us, length us, event | category | flops | bytes accessed | tf_op | source)
XLA Modules:
  0.0 114.4 jit_solution(16729290940814623827)
XLA Ops:
  7.2 0.0 copy-start
  7.2 0.0 copy-start.8
  7.2 0.0 copy-start.11
  7.2 0.0 copy-start.4
  7.2 0.0 reduce-scatter.2.cloned.1.call-start
  7.3 1.3 %copy-done = bf16[512,1536]{1,0:T(8,128)(2,1)S(1)} copy-done((bf16[512,1536]{1,0:T(8,128)(2,1)S(1)}, bf16[512,1536]{1,0:T(8,128)(2,1)}, u32[]{:S(2)}) %copy-start) | copy-done | bytes 1572888
  8.6 0.0 copy-start.5
  8.6 1.1 fusion.70
  9.7 0.0 copy-done.8
  9.7 0.0 copy-done.11
  9.7 0.0 copy-done.4
  9.8 0.0 copy-start.6
  9.8 0.3 fusion.68
  10.1 0.1 copy-done.5
  10.1 0.3 fusion.66
  10.4 0.8 copy-done.6
  11.3 0.0 copy-start.13
  11.3 0.3 fusion.64
  11.6 0.0 copy-start.12
  11.6 0.0 copy-start.1
  11.6 0.8 pad_maximum_fusion
  12.4 0.0 reduce-scatter.2.cloned.1.call-update
  12.4 0.0 all-reduce.2.cloned.1.call-start
  12.4 0.0 copy-done.13
  12.4 0.2 fusion.26
  12.6 0.1 fusion.22
  12.8 0.1 fusion.23
  12.9 0.1 fusion.24
  13.0 0.2 fusion.27
  14.5 0.1 copy.29
  14.6 0.1 fusion.52
  14.7 13.6 %psum.21 = f32[16]{0:T(128)S(1)} all-reduce(f32[16]{0:T(128)S(1)} %fusion.52), channel_id=1, replica_groups=mesh['dp'=4,'kv'=4,'tp'=2] {'kv'}, use_global_device_ids=true, to_apply=%region_2.0 | all-reduce | flops 16 | bytes 128 | tf_op jit(solution)/shard_map/psum | solution.py:60
  28.4 7.6 %reduce-scatter.2.cloned.1.call-done = f32[16,1536]{1,0:T(8,128)} async-done(((f32[16,6144]{1,0:T(8,128)}), f32[16,1536]{1,0:T(8,128)}) %reduce-scatter.2.cloned.1.call-update) | async-done | bytes 98320 | tf_op jit(solution)/shard_map/reduce_scatter | solution.py:61
  36.0 1.0 multiply_convert_fusion
  37.0 13.6 %all_gather.6 = bf16[16,6144]{1,0:T(8,128)(2,1)S(1)} all-gather(bf16[16,1536]{1,0:T(8,128)(2,1)S(1)} %multiply_convert_fusion), channel_id=1, replica_groups=mesh['dp'=4,'kv'=4,'tp'=2] {'kv'}, dimensions={1}, use_global_device_ids=true | all-gather | bytes 245760 | tf_op jit(solution)/shard_map/all_gather | solution.py:63
  50.6 0.9 reshape.356
  51.4 0.9 fusion.80
  52.4 0.0 copy-done.12
  52.4 0.2 fusion.45
  52.5 0.0 copy-done.1
  52.5 0.0 copy-start.9
  52.6 0.5 fusion.32
  53.1 0.3 fusion.31
  53.4 13.2 %all-gather.1 = f32[4,12,16]{2,1,0:T(8,128)S(1)} all-gather(f32[1,12,16]{2,1,0:T(8,128)S(1)} %bitcast.103), channel_id=2, replica_groups=mesh['dp'=4,'kv'=4,'tp'=2] {'kv'}, dimensions={0}, use_global_device_ids=true | all-gather | bytes 3840 | tf_op jit(solution)/shard_map/all_gather | solution.py:91
  66.6 0.1 fusion.53
  66.6 0.1 fusion.43
  66.7 0.0 copy-start.2
  66.8 0.9 fusion.13
  67.7 0.0 copy-done.9
  67.7 0.5 copy-done.2
  68.2 1.0 fusion.14
  69.1 0.0 all-reduce.2.cloned.1.call-update
  69.1 0.0 copy-start.3
  69.2 1.8 %bitcast_select_fusion.1 = bf16[1,512,12,128]{3,1,2,0:T(8,128)(2,1)} fusion(bf16[1,512,12,128]{3,1,2,0:T(8,128)(2,1)S(1)} %copy-done.1, pred[512]{0:T(512)(128)(4,1)S(1)} %compare_and_fusion, bf16[1,16,1,12,128]{4,3,2,1,0:T(8,128)(2,1)S(1)} %get-tuple-element.4, s32[512]{0:T(512)S(1)} %fusion.73), kind=kOutput, calls=%fused_computation.3 | convolution fusion | flops 26746880 | bytes 3197440 | tf_op jit(solution)/shard_map/scp,sphd->schd/dot_general | solution.py:118
  70.9 0.0 copy-done.3
  70.9 0.0 copy-start.10
  70.9 1.8 %bitcast_select_fusion = bf16[1,512,12,128]{3,1,2,0:T(8,128)(2,1)} fusion(bf16[1,512,12,128]{3,1,2,0:T(8,128)(2,1)S(1)} %copy-done.3, pred[512]{0:T(512)(128)(4,1)S(1)} %compare_and_fusion, bf16[1,16,1,12,128]{4,3,2,1,0:T(8,128)(2,1)S(1)} %get-tuple-element.3, s32[512]{0:T(512)S(1)} %fusion.73), kind=kOutput, calls=%fused_computation.2 | convolution fusion | flops 26746880 | bytes 3197440 | tf_op jit(solution)/shard_map/scp,sphd->schd/dot_general | solution.py:121
  72.7 0.0 copy-done.10
  72.7 0.3 fusion.21
  73.0 29.2 %all-reduce.2.cloned.1.call-done = f32[1,16,12,128]{3,1,2,0:T(8,128)} async-done(((f32[1,16,12,128]{3,1,2,0:T(8,128)}), f32[1,16,12,128]{3,1,2,0:T(8,128)}) %all-reduce.2.cloned.1.call-update) | async-done | bytes 98320 | tf_op jit(solution)/shard_map/psum | solution.py:105
  102.2 1.1 fusion.17
  103.3 0.0 copy-done.7
  103.3 0.3 convolution_convert_fusion.2
  103.6 4.0 %psum.23 = bf16[1,16,512]{2,1,0:T(8,128)(2,1)} all-reduce(bf16[1,16,512]{2,1,0:T(8,128)(2,1)S(1)} %bitcast.102), channel_id=1, replica_groups=mesh['dp'=4,'kv'=4,'tp'=2] {'tp'}, use_global_device_ids=true, to_apply=%region_7.8 | all-reduce | flops 8192 | bytes 32768 | tf_op jit(solution)/shard_map/psum | solution.py:112
  (8 shorter events, 0.1 us)
Async XLA Ops:
  7.2 1.4 %copy-start = (bf16[512,1536]{1,0:T(8,128)(2,1)S(1)}, bf16[512,1536]{1,0:T(8,128)(2,1)}, u32[]{:S(2)}) copy-start(bf16[512,1536]{1,0:T(8,128)(2,1)} %param.15) | copy-start | bytes 4718596
  7.2 2.5 %copy-start.8 = (bf16[1,16,512]{2,1,0:T(8,128)(2,1)S(1)}, bf16[1,16,512]{2,1,0:T(8,128)(2,1)}, u32[]{:S(2)}) copy-start(bf16[1,16,512]{2,1,0:T(8,128)(2,1)} %param.13) | copy-start | bytes 49156
  7.2 2.5 %copy-start.11 = (f32[512]{0:T(512)S(1)}, f32[512]{0:T(512)}, u32[]{:S(2)}) copy-start(f32[512]{0:T(512)} %param.14) | copy-start | bytes 6148
  7.2 2.5 %copy-start.4 = (bf16[512,1536]{1,0:T(8,128)(2,1)S(1)}, bf16[512,1536]{1,0:T(8,128)(2,1)}, u32[]{:S(2)}) copy-start(bf16[512,1536]{1,0:T(8,128)(2,1)} %param.16) | copy-start | bytes 4718596
  7.2 28.8 %reduce-scatter.2.cloned.1.call-start = ((), (), s32[]{:S(2)}) async-start(), calls=%async_computation.1 | async-start | bytes 491520 | tf_op jit(solution)/shard_map/reduce_scatter | solution.py:61
  8.6 1.6 %copy-start.5 = (bf16[512,1536]{1,0:T(8,128)(2,1)S(1)}, bf16[512,1536]{1,0:T(8,128)(2,1)}, u32[]{:S(2)}) copy-start(bf16[512,1536]{1,0:T(8,128)(2,1)} %param.17) | copy-start | bytes 4718596
  9.8 1.5 %copy-start.6 = (bf16[512,1536]{1,0:T(8,128)(2,1)S(1)}, bf16[512,1536]{1,0:T(8,128)(2,1)}, u32[]{:S(2)}) copy-start(bf16[512,1536]{1,0:T(8,128)(2,1)} %param.18) | copy-start | bytes 4718596
  11.3 1.2 %copy-start.13 = (s32[1,16]{1,0:T(1,128)S(1)}, s32[1,16]{1,0:T(1,128)}, u32[]{:S(2)}) copy-start(s32[1,16]{1,0:T(1,128)} %param.25) | copy-start | bytes 196
  11.6 40.8 %copy-start.12 = (f32[12]{0:T(128)S(1)}, f32[12]{0:T(128)}, u32[]{:S(2)}) copy-start(f32[12]{0:T(128)} %param.20) | copy-start | bytes 148
  11.6 41.0 %copy-start.1 = (bf16[1,512,12,128]{3,1,2,0:T(8,128)(2,1)S(1)}, bf16[1,512,12,128]{3,1,2,0:T(8,128)(2,1)}, u32[]{:S(2)}) copy-start(bf16[1,512,12,128]{3,1,2,0:T(8,128)(2,1)} %param.21) | copy-start | bytes 4718596
  12.4 89.8 %all-reduce.2.cloned.1.call-start = ((), (), s32[]{:S(2)}) async-start(), calls=%async_computation.2 | async-start | bytes 196608 | tf_op jit(solution)/shard_map/psum | solution.py:105
  52.5 15.1 %copy-start.9 = (f32[12,16,16]{1,2,0:T(8,128)}, f32[12,16,16]{1,2,0:T(8,128)S(1)}, u32[]{:S(2)}) copy-start(f32[12,16,16]{1,2,0:T(8,128)S(1)} %get-tuple-element.9) | copy-start | bytes 36868
  66.7 1.4 %copy-start.2 = (bf16[1,512,12,128]{3,1,2,0:T(8,128)(2,1)S(1)}, bf16[1,512,12,128]{3,1,2,0:T(8,128)(2,1)}, u32[]{:S(2)}) copy-start(bf16[1,512,12,128]{3,1,2,0:T(8,128)(2,1)} %param.22) | copy-start | bytes 4718596
  69.1 1.8 %copy-start.3 = (bf16[1,512,12,128]{3,1,2,0:T(8,128)(2,1)S(1)}, bf16[1,512,12,128]{3,1,2,0:T(8,128)(2,1)}, u32[]{:S(2)}) copy-start(bf16[1,512,12,128]{3,1,2,0:T(8,128)(2,1)} %param.22) | copy-start | bytes 4718596
  70.9 1.8 %copy-start.10 = (f32[12,16,16]{1,2,0:T(8,128)S(1)}, f32[12,16,16]{1,2,0:T(8,128)}, u32[]{:S(2)}) copy-start(f32[12,16,16]{1,2,0:T(8,128)} %copy-done.9) | copy-start | bytes 36868
  70.9 32.4 %copy-start.7 = (bf16[1536,512]{1,0:T(8,128)(2,1)S(1)}, bf16[1536,512]{1,0:T(8,128)(2,1)}, u32[]{:S(2)}) copy-start(bf16[1536,512]{1,0:T(8,128)(2,1)} %param.19) | copy-start | bytes 4718596
Sparse Core Ops, SparseCore 0:
  12.5 23.4 reduce-scatter.1
  69.3 32.8 all-reduce.1
where the time goes:
time: 115 us; the launch traced here: 114 us
  blocking collectives  44.4 us (39%)
  waiting for transfers between devices  36.8 us (32%)
  between operations  15.6 us (14%)
  matrix products  10.6 us (9%)
  local copies, waits for them, and re-layouts  4.63 us (4%)
  other arithmetic  2.38 us (2%)
    psum x1, waiting for transfers between devices, local(): attended = lax.psum(local_sum, 'kv')  29.2 us
    psum x1, blocking collectives, local(): squares = lax.psum(square_part, 'kv')  13.6 us
    all_gather x1, blocking collectives, local(): lax.all_gather((share * rscale[:, None]).astype(jnp.bfloat16), 'kv', axis...  13.6 us
    all_gather x1, blocking collectives, local(): every = lax.all_gather(shard_rest[None], 'kv', axis=0, tiled=True)  13.2 us
    reduce_scatter x1, waiting for transfers between devices, local(): lax.psum_scatter(partial_value, 'kv', scatter_dimension=1, tiled=True)  7.6 us
    psum x1, blocking collectives, local(): lax.psum(part_out.astype(jnp.bfloat16), 'tp')  3.96 us
    unnamed x28, local copies, waits for them, and re-layouts  2.74 us
  transfers between devices with their start and end apart: 2, of which 2 were waited for; matrix products, arithmetic and copies ran while one was open for 4% of the time, Pallas kernels for 0%

commit v1 on v0

--- a/solution.py
+++ b/solution.py
@@ -102,7 +102,7 @@
     local_sum = jnp.einsum(
         "shpc,schd->sphd", cache_weight, cache_values, preferred_element_type=jnp.float32
     )
-    attended = lax.psum(local_sum, "kv")
+    attended = jnp.sum(lax.all_gather(local_sum, "kv"), axis=0)
     attended = attended + jnp.einsum(
         "shpj,sjhd->sphd", tree_weight, value_new, preferred_element_type=jnp.float32
     )

time: 115 us -> 101 us (0.88)
  waiting for transfers between devices: 36.8 us -> 7.76 us
  blocking collectives: 44.4 us -> 58.6 us
    psum x1 -> x0, waiting for transfers between devices: 29.2 us -> none  [local(): attended = lax.psum(local_sum, 'kv')]
    all_gather x0 -> x1, blocking collectives: none -> 14.2 us  [local(): attended = jnp.sum(lax.all_gather(local_sum, 'kv'), axis=0)]
    unnamed x28 -> x26, local copies, waits for them, and re-layouts: 2.74 us -> 2.74 us
  transfers between devices with their start and end apart: 2 -> 1, of which waited for: 2 -> 1; matrix products, arithmetic and copies ran while one was open for 4% -> 1% of each run, Pallas kernels for 0% -> 0%
where the time goes in v1:
time: 101 us
  blocking collectives  58.6 us (58%)
  between operations  15.5 us (15%)
  matrix products  11.4 us (11%)
  waiting for transfers between devices  7.76 us (8%)
  local copies, waits for them, and re-layouts  4.63 us (5%)
  other arithmetic  3.04 us (3%)
    all_gather x1, blocking collectives, local(): attended = jnp.sum(lax.all_gather(local_sum, 'kv'), axis=0)  14.2 us
    all_gather x1, blocking collectives, local(): lax.all_gather((share * rscale[:, None]).astype(jnp.bfloat16), 'kv', axis...  13.6 us
    psum x1, blocking collectives, local(): squares = lax.psum(square_part, 'kv')  13.6 us
    all_gather x1, blocking collectives, local(): every = lax.all_gather(shard_rest[None], 'kv', axis=0, tiled=True)  13.2 us
    reduce_scatter x1, waiting for transfers between devices, local(): lax.psum_scatter(partial_value, 'kv', scatter_dimension=1, tiled=True)  7.74 us
    psum x1, blocking collectives, local(): lax.psum(part_out.astype(jnp.bfloat16), 'tp')  3.96 us
    unnamed x26, local copies, waits for them, and re-layouts  2.74 us
    dot_general x4, matrix products, local(): jnp.dot(scaled, weight, preferred_element_type=jnp.float32)  2.06 us
  transfers between devices with their start and end apart: 1, of which 1 were waited for; matrix products, arithmetic and copies ran while one was open for 1% of the time, Pallas kernels for 0%

profile of v1, /device:TPU:0, one launch (start us, length us, event | category | flops | bytes accessed | tf_op | source)
XLA Modules:
  0.0 101.0 jit_solution(7498128047702497777)
XLA Ops:
  7.2 0.0 copy-start
  7.2 0.0 copy-start.8
  7.2 0.0 copy-start.10
  7.2 0.0 copy-start.3
  7.2 0.0 reduce-scatter.2.cloned.1.call-start
  7.3 1.3 %copy-done = bf16[512,1536]{1,0:T(8,128)(2,1)S(1)} copy-done((bf16[512,1536]{1,0:T(8,128)(2,1)S(1)}, bf16[512,1536]{1,0:T(8,128)(2,1)}, u32[]{:S(2)}) %copy-start) | copy-done | bytes 1572888
  8.6 0.0 copy-start.4
  8.6 1.1 %fusion.70 = f32[16,1536]{1,0:T(8,128)S(1)} fusion(bf16[512,1536]{1,0:T(8,128)(2,1)S(1)} %copy-done, bf16[1,16,512]{2,1,0:T(8,128)(2,1)} %param.13, f32[512]{0:T(512)} %param.14), kind=kOutput, calls=%fused_computation.92 | convolution fusion | flops 25190400 | bytes 1689600 | tf_op jit(solution)/shard_map/dot_general | solution.py:55
  9.7 0.0 copy-done.8
  9.7 0.0 copy-done.10
  9.7 0.0 copy-done.3
  9.8 0.0 copy-start.5
  9.8 0.3 fusion.68
  10.1 0.1 copy-done.4
  10.1 0.3 fusion.66
  10.4 0.8 copy-done.5
  11.3 0.0 copy-start.12
  11.3 0.3 fusion.64
  11.6 0.0 copy-start.11
  11.6 0.8 pad_maximum_fusion
  12.4 0.0 copy-start.1
  12.4 0.0 reduce-scatter.2.cloned.1.call-update
  12.4 0.0 copy-done.12
  12.4 0.2 fusion.26
  12.6 0.1 fusion.22
  12.7 0.1 fusion.23
  12.9 0.1 fusion.24
  13.0 0.2 fusion.27
  14.5 0.1 copy.29
  14.5 0.1 fusion.52
  14.7 13.6 %psum.14 = f32[16]{0:T(128)S(1)} all-reduce(f32[16]{0:T(128)S(1)} %fusion.52), channel_id=1, replica_groups=mesh['dp'=4,'kv'=4,'tp'=2] {'kv'}, use_global_device_ids=true, to_apply=%region_2.0 | all-reduce | flops 16 | bytes 128 | tf_op jit(solution)/shard_map/psum | solution.py:60
  28.3 7.7 %reduce-scatter.2.cloned.1.call-done = f32[16,1536]{1,0:T(8,128)} async-done(((f32[16,6144]{1,0:T(8,128)}), f32[16,1536]{1,0:T(8,128)}) %reduce-scatter.2.cloned.1.call-update) | async-done | bytes 98320 | tf_op jit(solution)/shard_map/reduce_scatter | solution.py:61
  36.1 1.0 multiply_convert_fusion
  37.0 13.6 %all_gather.12 = bf16[16,6144]{1,0:T(8,128)(2,1)S(1)} all-gather(bf16[16,1536]{1,0:T(8,128)(2,1)S(1)} %multiply_convert_fusion), channel_id=1, replica_groups=mesh['dp'=4,'kv'=4,'tp'=2] {'kv'}, dimensions={1}, use_global_device_ids=true | all-gather | bytes 245760 | tf_op jit(solution)/shard_map/all_gather | solution.py:63
  50.7 0.0 copy-start.7
  50.7 0.9 reshape.357
  51.5 0.9 fusion.80
  52.4 0.0 copy-start.9
  52.4 0.0 copy-done.11
  52.5 0.2 fusion.45
  52.6 0.1 fusion.43
  52.7 0.9 fusion.21
  53.6 0.0 copy-done.1
  53.6 0.5 fusion.32
  54.1 0.0 copy-done.7
  54.1 0.3 fusion.31
  54.5 13.2 %all-gather.2 = f32[4,12,16]{2,1,0:T(8,128)S(1)} all-gather(f32[1,12,16]{2,1,0:T(8,128)S(1)} %bitcast.105), channel_id=2, replica_groups=mesh['dp'=4,'kv'=4,'tp'=2] {'kv'}, dimensions={0}, use_global_device_ids=true | all-gather | bytes 3840 | tf_op jit(solution)/shard_map/all_gather | solution.py:91
  67.6 0.1 fusion.53
  67.7 0.0 copy-start.2
  67.7 0.9 fusion.13
  68.7 0.5 copy-done.2
  69.1 0.3 fusion.14
  69.5 14.2 %all-gather.1 = f32[4,16,12,128]{3,1,2,0:T(8,128)S(1)} all-gather(f32[1,16,12,128]{3,1,2,0:T(8,128)S(1)} %fusion.14), channel_id=3, replica_groups=mesh['dp'=4,'kv'=4,'tp'=2] {'kv'}, dimensions={0}, use_global_device_ids=true | all-gather | bytes 491520 | tf_op jit(solution)/shard_map/all_gather | solution.py:105
  83.7 1.8 %bitcast_select_fusion.1 = bf16[1,512,12,128]{3,1,2,0:T(8,128)(2,1)} fusion(bf16[1,512,12,128]{3,1,2,0:T(8,128)(2,1)S(1)} %copy-done.1, pred[512]{0:T(512)(128)(4,1)S(1)} %compare_and_fusion, bf16[1,16,1,12,128]{4,3,2,1,0:T(8,128)(2,1)S(1)} %get-tuple-element.4, s32[512]{0:T(512)S(1)} %fusion.73), kind=kOutput, calls=%fused_computation.3 | convolution fusion | flops 26746880 | bytes 3197440 | tf_op jit(solution)/shard_map/scp,sphd->schd/dot_general | solution.py:118
  85.5 0.0 copy-done.9
  85.5 0.0 copy-start.6
  85.5 1.8 %bitcast_select_fusion = bf16[1,512,12,128]{3,1,2,0:T(8,128)(2,1)} fusion(bf16[1,512,12,128]{3,1,2,0:T(8,128)(2,1)S(1)} %copy-done.2, pred[512]{0:T(512)(128)(4,1)S(1)} %compare_and_fusion, bf16[1,16,1,12,128]{4,3,2,1,0:T(8,128)(2,1)S(1)} %get-tuple-element.3, s32[512]{0:T(512)S(1)} %fusion.73), kind=kOutput, calls=%fused_computation.2 | convolution fusion | flops 26746880 | bytes 3197440 | tf_op jit(solution)/shard_map/scp,sphd->schd/dot_general | solution.py:121
  87.2 0.7 reduce.6
  87.9 1.2 %fusion.17 = f32[1,16,12,128]{3,1,2,0:T(8,128)S(1)} fusion(bf16[12,16,16]{1,2,0:T(8,128)(2,1)} %fusion.21, f32[16,12,128]{2,0,1:T(8,128)} %reduce.6, bf16[1,16,1,12,128]{4,3,2,1,0:T(8,128)(2,1)} %copy-done.9), kind=kOutput, calls=%fused_computation.18 | convolution fusion | flops 811008 | bytes 251904 | tf_op jit(solution)/shard_map/shpj,sjhd->sphd/dot_general | solution.py:106
  89.1 0.0 copy-done.6
  89.1 1.1 %convolution_convert_fusion.2 = bf16[16,512]{1,0:T(8,128)(2,1)S(1)} fusion(bf16[1536,512]{1,0:T(8,128)(2,1)S(1)} %copy-done.6, f32[2,8,12,128]{3,2,1,0:T(8,128)S(1)} %bitcast.103, bf16[16,6144]{1,0:T(8,128)(2,1)} %copy-done.7), kind=kOutput, calls=%fused_computation.25 | convolution fusion | flops 25346048 | bytes 1736704 | tf_op jit(solution)/shard_map/dot_general | solution.py:110
  90.2 4.0 %psum.15 = bf16[1,16,512]{2,1,0:T(8,128)(2,1)} all-reduce(bf16[1,16,512]{2,1,0:T(8,128)(2,1)S(1)} %bitcast.104), channel_id=1, replica_groups=mesh['dp'=4,'kv'=4,'tp'=2] {'tp'}, use_global_device_ids=true, to_apply=%region_7.8 | all-reduce | flops 8192 | bytes 32768 | tf_op jit(solution)/shard_map/psum | solution.py:112
  (7 shorter events, 0.1 us)
Async XLA Ops:
  7.2 1.4 %copy-start = (bf16[512,1536]{1,0:T(8,128)(2,1)S(1)}, bf16[512,1536]{1,0:T(8,128)(2,1)}, u32[]{:S(2)}) copy-start(bf16[512,1536]{1,0:T(8,128)(2,1)} %param.15) | copy-start | bytes 4718596
  7.2 2.5 %copy-start.8 = (bf16[1,16,512]{2,1,0:T(8,128)(2,1)S(1)}, bf16[1,16,512]{2,1,0:T(8,128)(2,1)}, u32[]{:S(2)}) copy-start(bf16[1,16,512]{2,1,0:T(8,128)(2,1)} %param.13) | copy-start | bytes 49156
  7.2 2.5 %copy-start.10 = (f32[512]{0:T(512)S(1)}, f32[512]{0:T(512)}, u32[]{:S(2)}) copy-start(f32[512]{0:T(512)} %param.14) | copy-start | bytes 6148
  7.2 2.5 %copy-start.3 = (bf16[512,1536]{1,0:T(8,128)(2,1)S(1)}, bf16[512,1536]{1,0:T(8,128)(2,1)}, u32[]{:S(2)}) copy-start(bf16[512,1536]{1,0:T(8,128)(2,1)} %param.16) | copy-start | bytes 4718596
  7.2 28.9 %reduce-scatter.2.cloned.1.call-start = ((), (), s32[]{:S(2)}) async-start(), calls=%async_computation.1 | async-start | bytes 491520 | tf_op jit(solution)/shard_map/reduce_scatter | solution.py:61
  8.6 1.6 %copy-start.4 = (bf16[512,1536]{1,0:T(8,128)(2,1)S(1)}, bf16[512,1536]{1,0:T(8,128)(2,1)}, u32[]{:S(2)}) copy-start(bf16[512,1536]{1,0:T(8,128)(2,1)} %param.17) | copy-start | bytes 4718596
  9.8 1.5 %copy-start.5 = (bf16[512,1536]{1,0:T(8,128)(2,1)S(1)}, bf16[512,1536]{1,0:T(8,128)(2,1)}, u32[]{:S(2)}) copy-start(bf16[512,1536]{1,0:T(8,128)(2,1)} %param.18) | copy-start | bytes 4718596
  11.3 1.1 %copy-start.12 = (s32[1,16]{1,0:T(1,128)S(1)}, s32[1,16]{1,0:T(1,128)}, u32[]{:S(2)}) copy-start(s32[1,16]{1,0:T(1,128)} %param.25) | copy-start | bytes 196
  11.6 40.9 %copy-start.11 = (f32[12]{0:T(128)S(1)}, f32[12]{0:T(128)}, u32[]{:S(2)}) copy-start(f32[12]{0:T(128)} %param.20) | copy-start | bytes 148
  12.4 41.2 %copy-start.1 = (bf16[1,512,12,128]{3,1,2,0:T(8,128)(2,1)S(1)}, bf16[1,512,12,128]{3,1,2,0:T(8,128)(2,1)}, u32[]{:S(2)}) copy-start(bf16[1,512,12,128]{3,1,2,0:T(8,128)(2,1)} %param.21) | copy-start | bytes 4718596
  50.7 3.5 %copy-start.7 = (bf16[16,6144]{1,0:T(8,128)(2,1)}, bf16[16,6144]{1,0:T(8,128)(2,1)S(1)}, u32[]{:S(2)}) copy-start(bf16[16,6144]{1,0:T(8,128)(2,1)S(1)} %all_gather.12) | copy-start | bytes 589828
  52.4 33.0 %copy-start.9 = (bf16[1,16,1,12,128]{4,3,2,1,0:T(8,128)(2,1)}, bf16[1,16,1,12,128]{4,3,2,1,0:T(8,128)(2,1)S(1)}, u32[]{:S(2)}) copy-start(bf16[1,16,1,12,128]{4,3,2,1,0:T(8,128)(2,1)S(1)} %get-tuple-element.3) | copy-start | bytes 147460
  67.7 1.4 %copy-start.2 = (bf16[1,512,12,128]{3,1,2,0:T(8,128)(2,1)S(1)}, bf16[1,512,12,128]{3,1,2,0:T(8,128)(2,1)}, u32[]{:S(2)}) copy-start(bf16[1,512,12,128]{3,1,2,0:T(8,128)(2,1)} %param.22) | copy-start | bytes 4718596
  85.5 3.6 %copy-start.6 = (bf16[1536,512]{1,0:T(8,128)(2,1)S(1)}, bf16[1536,512]{1,0:T(8,128)(2,1)}, u32[]{:S(2)}) copy-start(bf16[1536,512]{1,0:T(8,128)(2,1)} %param.19) | copy-start | bytes 4718596
Sparse Core Ops, SparseCore 0:
  12.5 23.5 reduce-scatter.1
